TPU v7x, 256 devices: a whole 4x4x8 slice. The times are simulated.
256 devices in a mesh: sp: 64 (over z, y, core), tp: 4 (over x).
Axes of the slice: x: 4, y: 4, z: 8, core: 2. Of those that a mesh axis runs over, the one named last changes fastest.
Arguments:
- queries: bfloat16 [8192, 2048], P('sp', 'tp'), may hold values from -6 to 6
- forget_logits: bfloat16 [2, 8192, 2048], P(None, 'sp', 'tp'), may hold values from -7.5 to 7.5
- value_matrix: bfloat16 [8192, 2048], P('sp', 'tp'), may hold values from -6 to 6
- output_gate_logits: bfloat16 [8192, 2048], P('sp', 'tp'), may hold values from -6 to 6
- forget_slack: float32 [2048], P('tp'), may hold values from 6.1035156e-05 to 0.07
- spike_log_forget: float32 [8192, 16], P('sp', 'tp'), may hold values from -2.8 to 0, as said below
- head_norm_gain: bfloat16 [128], replicated, may hold values from 0.099609375 to 1.8984375
- output_weight: bfloat16 [2048, 2048], P('tp'), may hold values from -0.125 to 0.125
- residual: bfloat16 [8192, 2048], P('sp'), may hold values from -6 to 6
- mixer_norm_gain: bfloat16 [2048], replicated, may hold values from 0.099609375 to 1.8984375
- mixer_gate_weight: bfloat16 [2048, 5632], P('sp', 'tp'), may hold values from -0.125 to 0.125
- mixer_up_weight: bfloat16 [2048, 5632], P('sp', 'tp'), may hold values from -0.125 to 0.125
- mixer_down_weight: bfloat16 [5632, 2048], P('tp', 'sp'), may hold values from -0.078125 to 0.078125
Outputs:
- layer_out: bfloat16 [8192, 2048], P(('sp', 'tp'))
Inputs may be any that keep to these rules, and one draw needn't show every extreme that they name: `spike_log_forget`: zero at all but a few tokens.
All inputs are finite; a program needn't handle non-finite values.
Results may differ from a plain program's by a relative error of at most 0.015.
Values may be sent and summed in bfloat16 or wider, within the bound.
No kernel may reach another device: no remote copies, remote signals or barrier semaphores. Data moves between devices by JAX's collectives and lax.ppermute only.
A program may use at most 128 MiB of HBM per device.

v0:
```python
import jax
import jax.numpy as jnp
from jax import lax
from jax.sharding import Mesh
from jax.sharding import PartitionSpec as P

BLOCK = 128
SP = ("sp_0", "sp_1", "sp_2")
SP_TP = ("sp_0", "sp_1", "sp_2", "tp")
NORM_EPS = 1e-06
BEST_PRECISION = lax.Precision.HIGHEST


def in_one_piece(arrays, axis, dim, along):
    both = jnp.concatenate(arrays, axis=along)
    whole, at, gathered = (lax.all_gather(both, axis, axis=dim, tiled=True), 0, [])
    for a in arrays:
        gathered.append(lax.slice_in_dim(whole, at, at + a.shape[along], axis=along))
        at += a.shape[along]
    return tuple(gathered)


def in_order(pieces, dim):
    dims = list(pieces.shape[1:])
    dims[dim] *= pieces.shape[0]
    return jnp.moveaxis(pieces, 0, dim).reshape(dims)


def gather_in_order(array, axes, order):
    pieces = array[None]
    for k in order:
        pieces = lax.all_gather(pieces, axes[k], axis=0, tiled=True)
    block = [lax.axis_size(axes[k]) for k in reversed(order)]
    pieces = pieces.reshape(*block, *array.shape)
    turned = sorted(range(len(order)), key=lambda place: order[len(order) - 1 - place])
    return pieces.transpose(*turned, *range(len(order), pieces.ndim)).reshape(-1, *array.shape)


def gathered_by_axis(array, axes, order, dim):
    return in_order(gather_in_order(array, axes, order), dim)


def neutral_like(array, identity):
    return jax.tree.map(
        lambda a, e: jnp.broadcast_to(jnp.asarray(e, a.dtype), a.shape), array, identity
    )


def carried_in(array, axes, combine, identity, reverse):
    before = start = neutral_like(array, identity)
    subtotal = array
    for axis in reversed(axes):
        size, position = (lax.axis_size(axis), lax.axis_index(axis))
        pieces = jax.tree.map(
            lambda part, kind: lax.all_gather(part.astype(kind), axis),
            subtotal,
            (jnp.bfloat16, jnp.bfloat16),
        )
        inside, subtotal = (start, start)
        for k in reversed(range(size)) if reverse else range(size):
            passed = k > position if reverse else k < position
            subtotal = combine(
                subtotal, jax.tree.map(lambda part, own: part[k].astype(own.dtype), pieces, array)
            )
            inside = jax.tree.map(lambda new, old: jnp.where(passed, new, old), subtotal, inside)
        before = combine(inside, before)
    return before


def in_blocks(array, dim, size):
    dims = array.shape
    pieces = array.reshape(*dims[:dim], size, dims[dim] // size, *dims[dim + 1 :])
    return jnp.moveaxis(pieces, dim, 0)


def summed_on_arrival(array, axis, dim):
    size = lax.axis_size(axis)
    pieces = lax.all_to_all(in_blocks(array, dim, size), axis, 0, 0, tiled=True)
    return jnp.sum(pieces.astype(jnp.float32), axis=0)


def from_everyone(array, axis):
    copies = jnp.broadcast_to(array, (lax.axis_size(axis), *array.shape))
    return lax.all_to_all(copies, axis, split_axis=0, concat_axis=0, tiled=True)


def gathered_copies(array, axis, dim):
    return in_order(from_everyone(array, axis), dim)


def rms_scale(entries, gain_vec):
    return (
        entries
        * lax.rsqrt(jnp.mean(entries * entries, axis=-1, keepdims=True) + NORM_EPS)
        * gain_vec.astype(jnp.float32)
    )


def reverse_rows(tensor):
    return jnp.flip(tensor, 0)


def local_sweep(query_f, key_f, decay_f, value_f):
    row_count, heads_present, head_width = query_f.shape
    blocks_count = row_count // BLOCK
    tri_mask = jnp.tril(jnp.ones((BLOCK, BLOCK), bool))

    def to_blocks(tensor):
        return tensor.reshape(blocks_count, BLOCK, heads_present, head_width)

    def advance(carried, segment):
        state_now, offset = carried
        query_seg, key_seg, decay_seg, value_seg = segment
        running = jnp.cumsum(decay_seg, axis=0)
        query_scaled = query_seg * jnp.exp(running)
        key_scaled = key_seg * jnp.exp(-running)
        scores = jnp.einsum("thd,shd->hts", query_scaled, key_scaled, precision=BEST_PRECISION)
        scores = jnp.where(tri_mask[None], scores, 0.0)
        result = jnp.einsum("hts,shv->thv", scores, value_seg, precision=BEST_PRECISION)
        result = result + jnp.einsum(
            "thd,hdv->thv", query_scaled, state_now, precision=BEST_PRECISION
        )
        final_log = running[-1]
        state_next = jnp.exp(final_log)[:, :, None] * state_now + jnp.einsum(
            "shd,shv->hdv",
            key_seg * jnp.exp(final_log[None] - running),
            value_seg,
            precision=BEST_PRECISION,
        )
        reach = query_seg * jnp.exp(running + offset)
        return ((state_next, offset + final_log), (result, reach))

    initial = (
        jnp.zeros((heads_present, head_width, head_width), jnp.float32),
        jnp.zeros((heads_present, head_width), jnp.float32),
    )
    (state_end, offset_end), (results, reaches) = lax.scan(
        advance,
        initial,
        (to_blocks(query_f), to_blocks(key_f), to_blocks(decay_f), to_blocks(value_f)),
    )
    shape_back = (row_count, heads_present, head_width)
    return (
        results.reshape(shape_back),
        reaches.reshape(shape_back),
        state_end,
        jnp.exp(offset_end),
    )


def chain(earlier, latter):
    return (earlier[0] * latter[0], latter[0][..., None] * earlier[1] + latter[1])


def local(
    queries,
    forget_logits,
    value_matrix,
    output_gate_logits,
    forget_slack,
    spike_log_forget,
    head_norm_gain,
    output_weight,
    residual,
    mixer_norm_gain,
    mixer_gate_weight,
    mixer_up_weight,
    mixer_down_weight,
):
    gate_whole, up_whole = in_one_piece((mixer_gate_weight, mixer_up_weight), SP, 0, 1)
    down_whole = gathered_by_axis(mixer_down_weight, SP, (1, 0, 2), 1)
    row_count = queries.shape[0]
    heads_present = spike_log_forget.shape[1]
    head_width = queries.shape[1] // heads_present
    query_f = (jax.nn.silu(queries.astype(jnp.float32)) * head_width ** (-0.5)).reshape(
        row_count, heads_present, head_width
    )
    value_f = value_matrix.astype(jnp.float32).reshape(row_count, heads_present, head_width)
    gate_random_key = (forget_slack * jax.nn.sigmoid(-forget_logits.astype(jnp.float32))).reshape(
        2, row_count, heads_present, head_width
    )
    decay_logarithm = jnp.log1p(-gate_random_key) + spike_log_forget[None, :, :, None]
    fore_local, fore_reach, fore_state, fore_total = local_sweep(
        query_f, gate_random_key[0], decay_logarithm[0], value_f
    )
    back_local, back_reach, back_state, back_total = local_sweep(
        reverse_rows(query_f),
        reverse_rows(gate_random_key[1]),
        reverse_rows(decay_logarithm[1]),
        reverse_rows(value_f),
    )
    neutral = (jnp.ones_like(fore_total), jnp.zeros_like(fore_state))
    _, fore_enter = carried_in((fore_total, fore_state), SP, chain, neutral, False)
    _, back_enter = carried_in((back_total, back_state), SP, chain, neutral, True)
    fore_out = fore_local + jnp.einsum(
        "thd,hdv->thv", fore_reach, fore_enter, precision=BEST_PRECISION
    )
    back_out = back_local + jnp.einsum(
        "thd,hdv->thv", back_reach, back_enter, precision=BEST_PRECISION
    )
    mixture = fore_out + reverse_rows(back_out)
    mixed = (
        rms_scale(mixture, head_norm_gain).reshape(row_count, heads_present * head_width)
        * jax.nn.silu(output_gate_logits.astype(jnp.float32))
    ).astype(jnp.bfloat16)
    part_rows = row_count // lax.axis_size("tp")
    own_start = lax.axis_index("tp") * part_rows
    partial_out = jnp.dot(mixed, output_weight, preferred_element_type=jnp.float32).astype(
        jnp.bfloat16
    )
    mixer_add = summed_on_arrival(
        lax.optimization_barrier(partial_out).astype(jnp.float32).astype(jnp.bfloat16), "tp", 0
    )
    own_resid = lax.dynamic_slice_in_dim(residual, own_start, part_rows, 0)
    hidden_state = (own_resid.astype(jnp.float32) + mixer_add).astype(jnp.bfloat16)
    normed_part = rms_scale(hidden_state.astype(jnp.float32), mixer_norm_gain).astype(jnp.bfloat16)
    normed = gathered_copies(normed_part, "tp", 0)
    gate_act = jnp.dot(normed, gate_whole, preferred_element_type=jnp.float32)
    up_act = jnp.dot(normed, up_whole, preferred_element_type=jnp.float32)
    inner = (jax.nn.silu(gate_act) * up_act).astype(jnp.bfloat16)
    lowered = jnp.dot(inner, down_whole, preferred_element_type=jnp.float32)
    lowered_term = lax.optimization_barrier(lowered.astype(jnp.bfloat16)).astype(jnp.float32)
    ffn_add = summed_on_arrival(lowered_term.astype(jnp.bfloat16), "tp", 0)
    return (hidden_state.astype(jnp.float32) + ffn_add).astype(jnp.bfloat16)


def solution(mesh):
    torus = Mesh(mesh.devices.reshape(8, 4, 2, mesh.shape["tp"]), ("sp_0", "sp_1", "sp_2", "tp"))
    return jax.shard_map(
        local,
        mesh=torus,
        in_specs=(
            P(SP, "tp"),
            P(None, SP, "tp"),
            P(SP, "tp"),
            P(SP, "tp"),
            P("tp"),
            P(SP, "tp"),
            P(),
            P("tp", None),
            P(SP, None),
            P(),
            P(SP, "tp"),
            P(SP, "tp"),
            P("tp", SP),
        ),
        out_specs=P(SP_TP, None),
        check_vma=False,
    )
```

profile of v0, /device:TPU:1, one launch (start us, length us, event | category | flops | bytes accessed | tf_op | source)
XLA Modules:
  0.0 290.6 jit_solution(12369992402076362102)
XLA Ops:
  6.5 12.1 %all-gather.2 = bf16[5632,32]{0,1:T(8,128)(2,1)S(1)} all-gather(bf16[1408,32]{0,1:T(8,128)(2,1)} %param.25), channel_id=4, replica_groups=mesh['sp_0'=8,'sp_1'=4,'sp_2'=2,'tp'=4] {'sp_1'}, dimensions={0}, use_global_device_ids=true | all-gather | bytes 450560 | tf_op jit(solution)/shard_map/all_gather | solution.py:32
  18.7 0.8 copy.172
  19.5 1.2 divide_multiply_fusion
  20.8 0.8 squeeze.39
  21.6 1.0 log1p.7
  22.6 0.8 copy.111
  23.4 1.2 broadcast_add_fusion
  24.7 1.0 fusion.40
  25.7 0.8 squeeze.37
  26.5 0.8 squeeze.43
  27.3 0.1 rev.19
  27.4 0.1 fusion.93
  27.6 0.1 fusion.276
  27.7 5.7 %all_gather.71 = bf16[2,4,128]{2,1,0:T(4,128)(2,1)S(1)} all-gather(bf16[1,4,128]{2,1,0:T(4,128)(2,1)S(1)} %get-tuple-element.86), channel_id=1, replica_groups=mesh['sp_0'=8,'sp_1'=4,'sp_2'=2,'tp'=4] {'sp_2'}, dimensions={0}, use_global_device_ids=true | all-gather | bytes 3072 | tf_op jit(solution)/shard_map/all_gather | solution.py:55
  33.4 6.6 %all_gather.72 = bf16[4,4,128]{2,1,0:T(4,128)(2,1)S(1)} all-gather(bf16[1,4,128]{2,1,0:T(4,128)(2,1)S(1)} %fusion.242), channel_id=1, replica_groups=mesh['sp_0'=8,'sp_1'=4,'sp_2'=2,'tp'=4] {'sp_1'}, dimensions={0}, use_global_device_ids=true | all-gather | bytes 5120 | tf_op jit(solution)/shard_map/all_gather | solution.py:55
  40.0 2.4 exponential_multiply_fusion.3
  42.5 0.6 fusion.16
  43.1 3.6 %all-gather.1 = bf16[8,128,128]{2,1,0:T(8,128)(2,1)S(1)} all-gather(bf16[4,128,128]{2,1,0:T(8,128)(2,1)S(1)} %fusion.16), channel_id=3, replica_groups=mesh['sp_0'=8,'sp_1'=4,'sp_2'=2,'tp'=4] {'sp_2'}, dimensions={0}, use_global_device_ids=true | all-gather | bytes 393216 | tf_op jit(solution)/shard_map/all_gather | solution.py:55
  46.7 0.6 fusion.251
  47.4 0.2 fusion.88
  47.6 11.1 %all_gather.76 = bf16[4,4,128,128]{3,2,1,0:T(8,128)(2,1)S(1)} all-gather(bf16[1,4,128,128]{3,2,1,0:T(8,128)(2,1)S(1)} %fusion.88), channel_id=1, replica_groups=mesh['sp_0'=8,'sp_1'=4,'sp_2'=2,'tp'=4] {'sp_1'}, dimensions={0}, use_global_device_ids=true | all-gather | bytes 655360 | tf_op jit(solution)/shard_map/all_gather | solution.py:55
  58.7 0.6 copy-done.11
  59.3 1.0 fusion.74
  60.4 3.5 %all_gather.64 = bf16[2,4,128]{2,1,0:T(4,128)(2,1)S(1)} all-gather(bf16[1,4,128]{2,1,0:T(4,128)(2,1)S(1)} %get-tuple-element.113), channel_id=1, replica_groups=mesh['sp_0'=8,'sp_1'=4,'sp_2'=2,'tp'=4] {'sp_2'}, dimensions={0}, use_global_device_ids=true | all-gather | bytes 3072 | tf_op jit(solution)/shard_map/all_gather | solution.py:55
  63.9 5.9 %all_gather.65 = bf16[4,4,128]{2,1,0:T(4,128)(2,1)S(1)} all-gather(bf16[1,4,128]{2,1,0:T(4,128)(2,1)S(1)} %fusion.240), channel_id=1, replica_groups=mesh['sp_0'=8,'sp_1'=4,'sp_2'=2,'tp'=4] {'sp_1'}, dimensions={0}, use_global_device_ids=true | all-gather | bytes 5120 | tf_op jit(solution)/shard_map/all_gather | solution.py:55
  69.9 0.7 exponential_multiply_fusion.7
  70.6 1.4 fusion.15
  71.9 3.7 %all-gather = bf16[8,128,128]{2,1,0:T(8,128)(2,1)S(1)} all-gather(bf16[4,128,128]{2,1,0:T(8,128)(2,1)S(1)} %fusion.15), channel_id=2, replica_groups=mesh['sp_0'=8,'sp_1'=4,'sp_2'=2,'tp'=4] {'sp_2'}, dimensions={0}, use_global_device_ids=true | all-gather | bytes 393216 | tf_op jit(solution)/shard_map/all_gather | solution.py:55
  75.7 0.7 fusion.246
  76.4 0.2 fusion.84
  76.6 9.9 %all_gather.69 = bf16[4,4,128,128]{3,2,1,0:T(8,128)(2,1)S(1)} all-gather(bf16[1,4,128,128]{3,2,1,0:T(8,128)(2,1)S(1)} %fusion.84), channel_id=1, replica_groups=mesh['sp_0'=8,'sp_1'=4,'sp_2'=2,'tp'=4] {'sp_1'}, dimensions={0}, use_global_device_ids=true | all-gather | bytes 655360 | tf_op jit(solution)/shard_map/all_gather | solution.py:55
  86.5 0.8 copy-done.1
  87.3 1.0 fusion.56
  88.4 0.5 all-gather.17.cloned.1.call-update
  89.0 1.6 pad_maximum_fusion
  90.6 1.2 convert_element_type.813
  91.9 15.8 %all_gather.73 = bf16[8,4,128]{2,1,0:T(4,128)(2,1)S(1)} all-gather(bf16[1,4,128]{2,1,0:T(4,128)(2,1)S(1)} %fusion.252), channel_id=1, replica_groups=mesh['sp_0'=8,'sp_1'=4,'sp_2'=2,'tp'=4] {'sp_0'}, dimensions={0}, use_global_device_ids=true | all-gather | bytes 9216 | tf_op jit(solution)/shard_map/all_gather | solution.py:55
  107.7 9.8 %all_gather.66 = bf16[8,4,128]{2,1,0:T(4,128)(2,1)S(1)} all-gather(bf16[1,4,128]{2,1,0:T(4,128)(2,1)S(1)} %fusion.247), channel_id=1, replica_groups=mesh['sp_0'=8,'sp_1'=4,'sp_2'=2,'tp'=4] {'sp_0'}, dimensions={0}, use_global_device_ids=true | all-gather | bytes 9216 | tf_op jit(solution)/shard_map/all_gather | solution.py:55
  117.6 0.6 fusion.259
  118.2 0.6 fusion.266
  118.8 1.6 convolution_select_fusion.1
  120.4 0.4 convolution_bitcast_fusion.5
  120.9 1.6 convolution_select_fusion
  122.5 0.6 convolution_bitcast_fusion.2
  123.2 1.4 fusion.11
  124.5 1.4 fusion.14
  125.9 4.2 %fusion.10 = f32[128,4,128]{0,2,1:T(8,128)} fusion(f32[128,4,128]{0,2,1:T(8,128)} %fusion.11, f32[128,4,128]{2,1,0:T(4,128)S(1)} %get-tuple-element.68, bf16[8,4,128,128]{3,2,1,0:T(8,128)(2,1)} %all-gather.11.cloned.1.call-done, f32[4,128]{1,0:T(4,128)S(1)} %get-tuple-element.110, f32[4,128]{1,0:T(4,128)} %copy-done.7, f32[4,128]{1,0:T(4,128)} %copy-done.9, ...), kind=kOutput, calls=%fused_computation.9 | convolution fusion | flops 104464384 | bytes 2654222 | tf_op jit(solution)/shard_map/thd,hdv->thv/dot_general | solution.py:198
  130.2 2.0 rev.20
  132.1 7.9 %all-gather.9.cloned.1.call-done = bf16[8,4,128,128]{3,2,1,0:T(8,128)(2,1)} async-done(((bf16[1,4,128,128]{3,2,1,0:T(8,128)(2,1)}), bf16[8,4,128,128]{3,2,1,0:T(8,128)(2,1)}) %all-gather.9.cloned.1.call-update) | async-done | bytes 1048592 | tf_op jit(solution)/shard_map/all_gather | solution.py:55
  140.1 3.7 %multiply_reduce_fusion = (f32[128,4]{0,1:T(4,128)S(1)}, f32[128,4,128]{0,2,1:T(8,128)S(1)}) fusion(f32[128,4,128]{0,2,1:T(8,128)S(1)} %rev.20, f32[128,4,128]{0,2,1:T(8,128)} %fusion.14, f32[128,4,128]{2,1,0:T(4,128)S(1)} %get-tuple-element.67, bf16[8,4,128,128]{3,2,1,0:T(8,128)(2,1)} %all-gather.9.cloned.1.call-done, ...), kind=kOutput, calls=%fused_computation.172 | convolution fusion | flops 104660480 | bytes 2918414 | tf_op jit(solution)/shard_map/thd,hdv->thv/dot_general | solution.py:195
  143.8 0.1 copy.130
  144.0 1.3 convolution_convert_fusion
  145.3 3.9 %all-to-all-start = ((bf16[4,32,2048]{2,1,0:T(8,128)(2,1)}), bf16[4,32,2048]{2,1,0:T(8,128)(2,1)S(1)}, u32[]{:S(2)}, u32[]{:S(2)}) async-start(bf16[4,32,2048]{2,1,0:T(8,128)(2,1)} %bitcast.67), calls=%async_computation | async-start | bytes 1048576 | tf_op jit(solution)/shard_map/all_to_all | solution.py:78
  149.2 6.9 %all-to-all-done = bf16[4,32,2048]{2,1,0:T(8,128)(2,1)S(1)} async-done(((bf16[4,32,2048]{2,1,0:T(8,128)(2,1)}), bf16[4,32,2048]{2,1,0:T(8,128)(2,1)S(1)}, u32[]{:S(2)}, u32[]{:S(2)}) %all-to-all-start) | async-done | bytes 524320 | tf_op jit(solution)/shard_map/all_to_all | solution.py:78
  156.2 1.1 fusion.89
  157.4 0.9 broadcast_in_dim.106
  158.3 3.7 %all-to-all-start.1 = ((bf16[4,32,2048]{2,1,0:T(8,128)(2,1)}), bf16[4,32,2048]{2,1,0:T(8,128)(2,1)S(1)}, u32[]{:S(2)}, u32[]{:S(2)}) async-start(bf16[4,32,2048]{2,1,0:T(8,128)(2,1)} %broadcast_in_dim.106), calls=%async_computation.1 | async-start | bytes 1048576 | tf_op jit(solution)/shard_map/all_to_all | solution.py:84
  162.0 5.2 %all-gather.17.cloned.1.call-done = bf16[64,1408,32]{1,2,0:T(8,128)(2,1)} async-done(((bf16[32,1408,32]{1,2,0:T(8,128)(2,1)}), bf16[64,1408,32]{1,2,0:T(8,128)(2,1)}) %all-gather.17.cloned.1.call-update) | async-done | bytes 5767184 | tf_op jit(solution)/shard_map/all_gather | solution.py:32
  167.2 5.9 %copy.132 = bf16[8,4,2,1408,32]{3,4,2,1,0:T(8,128)(2,1)} copy(bf16[8,4,2,1408,32]{3,4,1,0,2:T(8,128)(2,1)} %bitcast.511) | data formatting | bytes 11534336 | tf_op jit(solution)/shard_map/transpose | solution.py:36
  173.1 85.4 %all-gather.13.cloned.1.call-done = bf16[2048,2816]{1,0:T(8,128)(2,1)} async-done(((bf16[32,2816]{1,0:T(8,128)(2,1)}), bf16[2048,2816]{1,0:T(8,128)(2,1)}) %all-gather.13.cloned.1.call-update) | async-done | bytes 11534352 | tf_op jit(solution)/shard_map/all_gather | solution.py:16
  258.5 4.5 %fusion.2 = f32[128,1408]{1,0:T(8,128)} fusion(bf16[128,2048]{1,0:T(8,128)(2,1)S(1)} %bitcast.516, bf16[2048,2816]{1,0:T(8,128)(2,1)} %all-gather.13.cloned.1.call-done), kind=kOutput, calls=%fused_computation.2 | convolution fusion | flops 738197504 | bytes 7012352 | tf_op jit(solution)/shard_map/dot_general | solution.py:218
  263.1 7.4 %convolution_convert_fusion.1 = bf16[128,2048]{1,0:T(8,128)(2,1)S(1)} fusion(bf16[1408,2048]{0,1:T(8,128)(2,1)} %bitcast.512, bf16[128,2048]{1,0:T(8,128)(2,1)S(1)} %bitcast.517, bf16[2048,2816]{1,0:T(8,128)(2,1)} %all-gather.13.cloned.1.call-done, f32[128,1408]{1,0:T(8,128)} %fusion.2), kind=kOutput, calls=%fused_computation.7 | convolution fusion | flops 1477738496 | bytes 13303808 | tf_op jit(solution)/shard_map/dot_general | solution.py:221
  270.5 12.8 %all_to_all.15 = bf16[4,32,2048]{2,1,0:T(8,128)(2,1)S(1)} all-to-all(bf16[4,32,2048]{2,1,0:T(8,128)(2,1)S(1)} %bitcast.518), channel_id=1, replica_groups=mesh['sp_0'=8,'sp_1'=4,'sp_2'=2,'tp'=4] {'tp'}, dimensions={0} | all-to-all | bytes 1048576 | tf_op jit(solution)/shard_map/all_to_all | solution.py:78
  283.4 0.7 fusion.92
  (88 shorter events, 1.0 us)
Async XLA Ops:
  6.5 137.5 %copy-start = (bf16[512,2048]{1,0:T(8,128)(2,1)S(1)}, bf16[512,2048]{1,0:T(8,128)(2,1)}, u32[]{:S(2)}) copy-start(bf16[512,2048]{1,0:T(8,128)(2,1)} %param.20) | copy-start | bytes 6291460
  6.5 20.7 %copy-start.2 = (bf16[128,512]{1,0:T(8,128)(2,1)S(1)}, bf16[128,512]{1,0:T(8,128)(2,1)}, u32[]{:S(2)}) copy-start(bf16[128,512]{1,0:T(8,128)(2,1)} %param.15) | copy-start | bytes 393220
  6.5 81.9 %all-gather.15.cloned.1.call-start = ((), (), s32[]{:S(2)}) async-start(), calls=%async_computation.6 | async-start | bytes 3244032 | tf_op jit(solution)/shard_map/all_gather | solution.py:32
  19.5 106.4 %all-gather.11.cloned.1.call-start = ((), (), s32[]{:S(2)}) async-start(), calls=%async_computation.4 | async-start | bytes 1179648 | tf_op jit(solution)/shard_map/all_gather | solution.py:55
  27.6 19.8 %copy-start.3 = (f32[128,4,128]{2,1,0:T(4,128)}, f32[128,4,128]{2,1,0:T(4,128)S(1)}, u32[]{:S(2)}) copy-start(f32[128,4,128]{2,1,0:T(4,128)S(1)} %fusion.93) | copy-start | bytes 786436
  46.7 0.7 copy-start.4
  46.7 17.2 %copy-start.7 = (f32[4,128]{1,0:T(4,128)}, f32[4,128]{1,0:T(4,128)S(1)}, u32[]{:S(2)}) copy-start(f32[4,128]{1,0:T(4,128)S(1)} %convert_bitcast_fusion.20) | copy-start | bytes 6148
  47.3 11.4 %copy-start.9 = (f32[4,128]{1,0:T(4,128)}, f32[4,128]{1,0:T(4,128)S(1)}, u32[]{:S(2)}) copy-start(f32[4,128]{1,0:T(4,128)S(1)} %get-tuple-element.105) | copy-start | bytes 6148
  58.7 0.6 copy-start.11
  58.7 0.6 copy-start.12
  58.7 0.6 copy-start.13
  60.3 79.7 %all-gather.9.cloned.1.call-start = ((), (), s32[]{:S(2)}) async-start(), calls=%async_computation.3 | async-start | bytes 1179648 | tf_op jit(solution)/shard_map/all_gather | solution.py:55
  75.7 0.7 copy-start.5
  75.7 10.8 %copy-start.8 = (f32[4,128]{1,0:T(4,128)}, f32[4,128]{1,0:T(4,128)S(1)}, u32[]{:S(2)}) copy-start(f32[4,128]{1,0:T(4,128)S(1)} %convert_bitcast_fusion.22) | copy-start | bytes 6148
  76.3 10.2 %copy-start.10 = (f32[4,128]{1,0:T(4,128)}, f32[4,128]{1,0:T(4,128)S(1)}, u32[]{:S(2)}) copy-start(f32[4,128]{1,0:T(4,128)S(1)} %get-tuple-element.101) | copy-start | bytes 6148
  86.5 0.8 copy-start.1
  86.5 0.8 copy-start.14
  86.5 0.8 copy-start.15
  86.5 0.8 copy-start.16
  88.3 78.8 %all-gather.17.cloned.1.call-start = ((), (), s32[]{:S(2)}) async-start(), calls=%async_computation.7 | async-start | bytes 8650752 | tf_op jit(solution)/shard_map/all_gather | solution.py:32
  88.9 169.6 %all-gather.13.cloned.1.call-start = ((), (), s32[]{:S(2)}) async-start(), calls=%async_computation.5 | async-start | bytes 11714560 | tf_op jit(solution)/shard_map/all_gather | solution.py:16
  120.9 19.1 %copy-start.18 = (f32[4,128]{1,0:T(4,128)S(1)}, f32[4,128]{1,0:T(4,128)}, u32[]{:S(2)}) copy-start(f32[4,128]{1,0:T(4,128)} %get-tuple-element.87) | copy-start | bytes 6148
  120.9 19.1 %copy-start.19 = (f32[4,128]{1,0:T(4,128)S(1)}, f32[4,128]{1,0:T(4,128)}, u32[]{:S(2)}) copy-start(f32[4,128]{1,0:T(4,128)} %get-tuple-element.88) | copy-start | bytes 6148
  120.9 19.1 %copy-start.20 = (f32[4,128]{1,0:T(4,128)S(1)}, f32[4,128]{1,0:T(4,128)}, u32[]{:S(2)}) copy-start(f32[4,128]{1,0:T(4,128)} %get-tuple-element.89) | copy-start | bytes 6148
  120.9 19.1 %copy-start.21 = (f32[4,128]{1,0:T(4,128)S(1)}, f32[4,128]{1,0:T(4,128)}, u32[]{:S(2)}) copy-start(f32[4,128]{1,0:T(4,128)} %get-tuple-element.90) | copy-start | bytes 6148
  120.9 19.1 %copy-start.22 = (f32[4,128]{1,0:T(4,128)S(1)}, f32[4,128]{1,0:T(4,128)}, u32[]{:S(2)}) copy-start(f32[4,128]{1,0:T(4,128)} %get-tuple-element.91) | copy-start | bytes 6148
  120.9 19.1 %copy-start.23 = (f32[4,128]{1,0:T(4,128)S(1)}, f32[4,128]{1,0:T(4,128)}, u32[]{:S(2)}) copy-start(f32[4,128]{1,0:T(4,128)} %get-tuple-element.92) | copy-start | bytes 6148
  120.9 19.1 %copy-start.24 = (f32[4,128]{1,0:T(4,128)S(1)}, f32[4,128]{1,0:T(4,128)}, u32[]{:S(2)}) copy-start(f32[4,128]{1,0:T(4,128)} %get-tuple-element.93) | copy-start | bytes 6148
  123.2 16.9 %copy-start.6 = (bf16[8,128,128]{2,1,0:T(8,128)(2,1)S(1)}, bf16[8,128,128]{2,1,0:T(8,128)(2,1)}, u32[]{:S(2)}) copy-start(bf16[8,128,128]{2,1,0:T(8,128)(2,1)} %copy-done.5) | copy-start | bytes 786436
  124.5 19.2 %copy-start.25 = (f32[128]{0:T(128)S(1)}, f32[128]{0:T(128)}, u32[]{:S(2)}) copy-start(f32[128]{0:T(128)} %convert_element_type.813) | copy-start | bytes 1540
  130.1 13.9 %copy-start.26 = (bf16[128,512]{1,0:T(8,128)(2,1)S(1)}, bf16[128,512]{1,0:T(8,128)(2,1)}, u32[]{:S(2)}) copy-start(bf16[128,512]{1,0:T(8,128)(2,1)} %param.16) | copy-start | bytes 393220
  130.1 19.1 %copy-start.17 = (bf16[2048]{0:T(1024)(128)(2,1)S(1)}, bf16[2048]{0:T(1024)(128)(2,1)}, u32[]{:S(2)}) copy-start(bf16[2048]{0:T(1024)(128)(2,1)} %param.22) | copy-start | bytes 12292
  145.3 10.9 %all-to-all-start = ((bf16[4,32,2048]{2,1,0:T(8,128)(2,1)}), bf16[4,32,2048]{2,1,0:T(8,128)(2,1)S(1)}, u32[]{:S(2)}, u32[]{:S(2)}) async-start(bf16[4,32,2048]{2,1,0:T(8,128)(2,1)} %bitcast.67), calls=%async_computation | async-start | bytes 1048576 | tf_op jit(solution)/shard_map/all_to_all | solution.py:78
  158.3 14.8 %all-to-all-start.1 = ((bf16[4,32,2048]{2,1,0:T(8,128)(2,1)}), bf16[4,32,2048]{2,1,0:T(8,128)(2,1)S(1)}, u32[]{:S(2)}, u32[]{:S(2)}) async-start(bf16[4,32,2048]{2,1,0:T(8,128)(2,1)} %broadcast_in_dim.106), calls=%async_computation.1 | async-start | bytes 1048576 | tf_op jit(solution)/shard_map/all_to_all | solution.py:84
Sparse Core Ops, SparseCore 0:
  19.6 45.9 all-gather.14
  67.4 33.8 all-gather.10
  103.2 36.8 all-gather.8
  141.7 25.4 all-gather.16
  169.8 88.7 all-gather.12
where the time goes:
time: 291 us
  waiting for transfers between devices  106 us (36%)
  blocking collectives  101 us (35%)
  matrix products  30.1 us (10%)
  other arithmetic  16.9 us (6%)
  local copies, waits for them, and re-layouts  15.6 us (5%)
  between operations  13.6 us (5%)
  starting transfers between devices  7.79 us (3%)
    all_gather x1, waiting for transfers between devices, in_one_piece(): lax.all_gather(both, axis, axis=dim, tiled=True)  85.4 us
    all_gather x10, blocking collectives, carried_in(): lax.all_gather(part.astype(kind), axis)  75.8 us
    all_to_all x1, blocking collectives, summed_on_arrival(): pieces = lax.all_to_all(in_blocks(array, dim, size), axis, 0, 0, tiled=True)  12.8 us
    all_gather x1, blocking collectives, gather_in_order(): pieces = lax.all_gather(pieces, axes[k], axis=0, tiled=True)  12.1 us
    all_gather x2, waiting for transfers between devices, carried_in(): lax.all_gather(part.astype(kind), axis)  7.87 us
    dot_general x1, matrix products, local(): lowered = jnp.dot(inner, down_whole, preferred_element_type=jnp.float32)  7.42 us
    all_to_all x1, waiting for transfers between devices, summed_on_arrival(): pieces = lax.all_to_all(in_blocks(array, dim, size), axis, 0, 0, tiled=True)  6.93 us
    transpose x1, local copies, waits for them, and re-layouts, gather_in_order(): pieces.transpose(*turned, *range(len(order), pieces.ndim))  5.92 us
  transfers between devices with their start and end apart: 7, of which 4 were waited for; matrix products, arithmetic and copies ran while one was open for 16% of the time, Pallas kernels for 0%

commit v1 on v0

--- a/solution.py
+++ b/solution.py
@@ -29,7 +29,9 @@
 def gather_in_order(array, axes, order):
     pieces = array[None]
     for k in order:
-        pieces = lax.all_gather(pieces, axes[k], axis=0, tiled=True)
+        pieces = jnp.concatenate(
+            lax.all_to_all(jnp.stack([pieces] * lax.axis_size(axes[k])), axes[k], 0, 0), axis=0
+        )
     block = [lax.axis_size(axes[k]) for k in reversed(order)]
     pieces = pieces.reshape(*block, *array.shape)
     turned = sorted(range(len(order)), key=lambda place: order[len(order) - 1 - place])

time: 291 us -> 305 us (1.048)
  waiting for transfers between devices: 106 us -> 81.9 us
  blocking collectives: 101 us -> 122 us
  local copies, waits for them, and re-layouts: 15.6 us -> 21.1 us
  other arithmetic: 16.9 us -> 22.4 us
  starting transfers between devices: 7.79 us -> 12.3 us
    all_gather x1, waiting for transfers between devices: 85.4 us -> 0.01 us  [in_one_piece(): lax.all_gather(both, axis, axis=dim, tiled=True)]
    all_to_all x1 -> x2, waiting for transfers between devices: 6.93 us -> 78.6 us  [gather_in_order(): lax.all_to_all(jnp.stack([pieces] * lax.axis_size(axes[k])), axes[k], 0, 0)]
    all_to_all x0 -> x1, blocking collectives: none -> 24.7 us  [gather_in_order(): lax.all_to_all(jnp.stack([pieces] * lax.axis_size(axes[k])), axes[k], 0, 0)]
    all_gather x1 -> x0, blocking collectives: 12.1 us -> none  [gather_in_order(): pieces = lax.all_gather(pieces, axes[k], axis=0, tiled=True)]
    all_to_all x1 -> x2, blocking collectives: 12.8 us -> 21.5 us  [summed_on_arrival(): pieces = lax.all_to_all(in_blocks(array, dim, size), axis, 0, 0, tiled=True)]
    all_gather x2, waiting for transfers between devices: 7.87 us -> 0.02 us  [carried_in(): lax.all_gather(part.astype(kind), axis)]
    all_to_all x0 -> x1, local copies, waits for them, and re-layouts: none -> 5.99 us  [gather_in_order(): lax.all_to_all(jnp.stack([pieces] * lax.axis_size(axes[k])), axes[k], 0, 0)]
    transpose x1 -> x0, local copies, waits for them, and re-layouts: 5.92 us -> none  [gather_in_order(): pieces.transpose(*turned, *range(len(order), pieces.ndim))]
  transfers between devices with their start and end apart: 7 -> 6, of which waited for: 4 -> 2; matrix products, arithmetic and copies ran while one was open for 16% -> 14% of each run, Pallas kernels for 0% -> 0%
where the time goes in v1:
time: 305 us; the launch traced here: 304 us
  blocking collectives  122 us (40%)
  waiting for transfers between devices  81.9 us (27%)
  matrix products  30.2 us (10%)
  other arithmetic  22.4 us (7%)
  local copies, waits for them, and re-layouts  21.1 us (7%)
  between operations  13.6 us (4%)
  starting transfers between devices  12.3 us (4%)
    all_to_all x2, waiting for transfers between devices, gather_in_order(): lax.all_to_all(jnp.stack([pieces] * lax.axis_size(axes[k])), axes[k], 0, 0)  78.6 us
    all_gather x10, blocking collectives, carried_in(): lax.all_gather(part.astype(kind), axis)  75.9 us
    all_to_all x1, blocking collectives, gather_in_order(): lax.all_to_all(jnp.stack([pieces] * lax.axis_size(axes[k])), axes[k], 0, 0)  24.7 us
    all_to_all x2, blocking collectives, summed_on_arrival(): pieces = lax.all_to_all(in_blocks(array, dim, size), axis, 0, 0, tiled=True)  21.5 us
    all_to_all x2, starting transfers between devices, gather_in_order(): lax.all_to_all(jnp.stack([pieces] * lax.axis_size(axes[k])), axes[k], 0, 0)  8.7 us
    dot_general x1, matrix products, local(): lowered = jnp.dot(inner, down_whole, preferred_element_type=jnp.float32)  7.42 us
  transfers between devices with their start and end apart: 6, of which 2 were waited for; matrix products, arithmetic and copies ran while one was open for 14% of the time, Pallas kernels for 0%

profile of v1, /device:TPU:1, one launch (start us, length us, event | category | flops | bytes accessed | tf_op | source)
XLA Modules:
  0.0 303.5 jit_solution(6444988574333195931)
XLA Ops:
  6.5 1.4 divide_multiply_fusion
  8.0 1.0 log1p.7
  8.9 0.8 copy.47
  9.7 1.2 broadcast_add_fusion
  11.1 0.8 rev.17
  11.9 1.1 fusion.276
  13.0 0.6 slice_bitcast_fusion.35
  13.6 4.7 %all_gather.62 = bf16[2,4,128]{2,1,0:T(4,128)(2,1)S(1)} all-gather(bf16[1,4,128]{2,1,0:T(4,128)(2,1)S(1)} %get-tuple-element.86), channel_id=1, replica_groups=mesh['sp_0'=8,'sp_1'=4,'sp_2'=2,'tp'=4] {'sp_2'}, dimensions={0}, use_global_device_ids=true | all-gather | bytes 3072 | tf_op jit(solution)/shard_map/all_gather | solution.py:57
  18.2 0.6 fusion.242
  18.8 0.7 fusion.275
  19.6 0.8 squeeze.39
  20.3 1.0 fusion.40
  21.3 0.8 squeeze.37
  22.1 1.7 squeeze.43
  24.0 6.5 %all_gather.63 = bf16[4,4,128]{2,1,0:T(4,128)(2,1)S(1)} all-gather(bf16[1,4,128]{2,1,0:T(4,128)(2,1)} %fusion.242), channel_id=1, replica_groups=mesh['sp_0'=8,'sp_1'=4,'sp_2'=2,'tp'=4] {'sp_1'}, dimensions={0}, use_global_device_ids=true | all-gather | bytes 5120 | tf_op jit(solution)/shard_map/all_gather | solution.py:57
  30.5 2.5 exponential_multiply_fusion.3
  33.0 0.6 fusion.16
  33.7 3.8 %all-gather.1 = bf16[8,128,128]{2,1,0:T(8,128)(2,1)S(1)} all-gather(bf16[4,128,128]{2,1,0:T(8,128)(2,1)S(1)} %fusion.16), channel_id=3, replica_groups=mesh['sp_0'=8,'sp_1'=4,'sp_2'=2,'tp'=4] {'sp_2'}, dimensions={0}, use_global_device_ids=true | all-gather | bytes 393216 | tf_op jit(solution)/shard_map/all_gather | solution.py:57
  37.5 0.6 fusion.251
  38.2 0.2 fusion.88
  38.4 9.9 %all_gather.67 = bf16[4,4,128,128]{3,2,1,0:T(8,128)(2,1)S(1)} all-gather(bf16[1,4,128,128]{3,2,1,0:T(8,128)(2,1)S(1)} %fusion.88), channel_id=1, replica_groups=mesh['sp_0'=8,'sp_1'=4,'sp_2'=2,'tp'=4] {'sp_1'}, dimensions={0}, use_global_device_ids=true | all-gather | bytes 655360 | tf_op jit(solution)/shard_map/all_gather | solution.py:57
  48.3 1.0 fusion.74
  49.4 5.4 %all_gather.55 = bf16[2,4,128]{2,1,0:T(4,128)(2,1)S(1)} all-gather(bf16[1,4,128]{2,1,0:T(4,128)(2,1)} %get-tuple-element.113), channel_id=1, replica_groups=mesh['sp_0'=8,'sp_1'=4,'sp_2'=2,'tp'=4] {'sp_2'}, dimensions={0}, use_global_device_ids=true | all-gather | bytes 3072 | tf_op jit(solution)/shard_map/all_gather | solution.py:57
  54.9 5.4 %all_gather.56 = bf16[4,4,128]{2,1,0:T(4,128)(2,1)S(1)} all-gather(bf16[1,4,128]{2,1,0:T(4,128)(2,1)S(1)} %fusion.240), channel_id=1, replica_groups=mesh['sp_0'=8,'sp_1'=4,'sp_2'=2,'tp'=4] {'sp_1'}, dimensions={0}, use_global_device_ids=true | all-gather | bytes 5120 | tf_op jit(solution)/shard_map/all_gather | solution.py:57
  60.2 0.7 exponential_multiply_fusion.7
  60.9 1.4 fusion.15
  62.3 3.6 %all-gather = bf16[8,128,128]{2,1,0:T(8,128)(2,1)S(1)} all-gather(bf16[4,128,128]{2,1,0:T(8,128)(2,1)S(1)} %fusion.15), channel_id=2, replica_groups=mesh['sp_0'=8,'sp_1'=4,'sp_2'=2,'tp'=4] {'sp_2'}, dimensions={0}, use_global_device_ids=true | all-gather | bytes 393216 | tf_op jit(solution)/shard_map/all_gather | solution.py:57
  65.9 0.7 fusion.246
  66.8 10.7 %all_gather.60 = bf16[4,4,128,128]{3,2,1,0:T(8,128)(2,1)S(1)} all-gather(bf16[1,4,128,128]{3,2,1,0:T(8,128)(2,1)S(1)} %fusion.84), channel_id=1, replica_groups=mesh['sp_0'=8,'sp_1'=4,'sp_2'=2,'tp'=4] {'sp_1'}, dimensions={0}, use_global_device_ids=true | all-gather | bytes 655360 | tf_op jit(solution)/shard_map/all_gather | solution.py:57
  77.6 0.7 copy-done.1
  78.3 1.0 fusion.56
  79.4 1.6 pad_maximum_fusion.1
  81.0 1.7 stack.9
  82.7 4.1 %all-to-all-start.2 = ((bf16[4,1,1408,32]{2,3,1,0:T(8,128)(2,1)}), bf16[4,1,1408,32]{2,3,1,0:T(8,128)(2,1)}, u32[]{:S(2)}, u32[]{:S(2)}) async-start(bf16[4,1,1408,32]{2,3,1,0:T(8,128)(2,1)} %stack.9), calls=%async_computation.2 | async-start | bytes 720896 | tf_op jit(solution)/shard_map/all_to_all | solution.py:33
  86.8 1.2 convert_element_type.813
  88.0 15.6 %all_gather.64 = bf16[8,4,128]{2,1,0:T(4,128)(2,1)S(1)} all-gather(bf16[1,4,128]{2,1,0:T(4,128)(2,1)S(1)} %fusion.252), channel_id=1, replica_groups=mesh['sp_0'=8,'sp_1'=4,'sp_2'=2,'tp'=4] {'sp_0'}, dimensions={0}, use_global_device_ids=true | all-gather | bytes 9216 | tf_op jit(solution)/shard_map/all_gather | solution.py:57
  103.6 10.3 %all_gather.57 = bf16[8,4,128]{2,1,0:T(4,128)(2,1)S(1)} all-gather(bf16[1,4,128]{2,1,0:T(4,128)(2,1)S(1)} %fusion.247), channel_id=1, replica_groups=mesh['sp_0'=8,'sp_1'=4,'sp_2'=2,'tp'=4] {'sp_0'}, dimensions={0}, use_global_device_ids=true | all-gather | bytes 9216 | tf_op jit(solution)/shard_map/all_gather | solution.py:57
  114.0 0.6 fusion.259
  114.6 0.6 fusion.266
  115.2 1.6 convolution_select_fusion.1
  116.8 0.4 convolution_bitcast_fusion.5
  117.3 1.6 convolution_select_fusion
  118.9 0.6 convolution_bitcast_fusion.2
  119.5 1.4 fusion.11
  120.9 1.4 fusion.14
  122.3 4.2 %fusion.10 = f32[128,4,128]{0,2,1:T(8,128)} fusion(f32[128,4,128]{0,2,1:T(8,128)} %fusion.11, f32[128,4,128]{2,1,0:T(4,128)S(1)} %get-tuple-element.68, bf16[8,4,128,128]{3,2,1,0:T(8,128)(2,1)} %all-gather.8.cloned.1.call-done, f32[4,128]{1,0:T(4,128)S(1)} %get-tuple-element.110, f32[4,128]{1,0:T(4,128)} %copy-done.7, f32[4,128]{1,0:T(4,128)} %copy-done.9, ...), kind=kOutput, calls=%fused_computation.10 | convolution fusion | flops 104464384 | bytes 2654222 | tf_op jit(solution)/shard_map/thd,hdv->thv/dot_general | solution.py:200
  126.5 1.9 rev.20
  128.5 3.7 %multiply_reduce_fusion = (f32[128,4]{0,1:T(4,128)S(1)}, f32[128,4,128]{0,2,1:T(8,128)S(1)}) fusion(f32[128,4,128]{0,2,1:T(8,128)S(1)} %rev.20, f32[128,4,128]{0,2,1:T(8,128)} %fusion.14, f32[128,4,128]{2,1,0:T(4,128)S(1)} %get-tuple-element.67, bf16[8,4,128,128]{3,2,1,0:T(8,128)(2,1)} %all-gather.6.cloned.1.call-done, ...), kind=kOutput, calls=%fused_computation.172 | convolution fusion | flops 104660480 | bytes 2918414 | tf_op jit(solution)/shard_map/thd,hdv->thv/dot_general | solution.py:197
  132.5 1.4 convolution_convert_fusion
  133.9 10.7 %all_to_all.30 = bf16[4,32,2048]{2,1,0:T(8,128)(2,1)S(1)} all-to-all(bf16[4,32,2048]{2,1,0:T(8,128)(2,1)S(1)} %bitcast.514), channel_id=1, replica_groups=mesh['sp_0'=8,'sp_1'=4,'sp_2'=2,'tp'=4] {'tp'}, dimensions={0} | all-to-all | bytes 1048576 | tf_op jit(solution)/shard_map/all_to_all | solution.py:80
  144.6 2.9 stack.10
  147.5 4.6 %all-to-all-start.3 = ((bf16[8,4,1408,32]{2,3,1,0:T(8,128)(2,1)}), bf16[8,4,1408,32]{2,3,1,0:T(8,128)(2,1)}, u32[]{:S(2)}, u32[]{:S(2)}) async-start(bf16[8,4,1408,32]{2,3,1,0:T(8,128)(2,1)} %stack.10), calls=%async_computation.3 | async-start | bytes 5767168 | tf_op jit(solution)/shard_map/all_to_all | solution.py:33
  152.2 1.1 fusion.89
  153.4 78.6 %all-to-all-done.3 = bf16[8,4,1408,32]{2,3,1,0:T(8,128)(2,1)} async-done(((bf16[8,4,1408,32]{2,3,1,0:T(8,128)(2,1)}), bf16[8,4,1408,32]{2,3,1,0:T(8,128)(2,1)}, u32[]{:S(2)}, u32[]{:S(2)}) %all-to-all-start.3) | async-done | bytes 2883616 | tf_op jit(solution)/shard_map/all_to_all | solution.py:33
  232.0 3.3 %pad_maximum_fusion = bf16[2,32,1408,32]{2,3,1,0:T(8,128)(2,1)S(1)} fusion(bf16[1,32,1408,32]{2,3,1,0:T(8,128)(2,1)} %bitcast.70), kind=kLoop, calls=%fused_computation.4 | loop fusion | flops 2883584 | bytes 8650752 | tf_op jit(solution)/shard_map/stack | solution.py:33
  235.3 24.7 %all_to_all.31 = bf16[2,32,1408,32]{2,3,1,0:T(8,128)(2,1)} all-to-all(bf16[2,32,1408,32]{2,3,1,0:T(8,128)(2,1)S(1)} %pad_maximum_fusion), channel_id=1, replica_groups=mesh['sp_0'=8,'sp_1'=4,'sp_2'=2,'tp'=4] {'sp_2'}, dimensions={0} | all-to-all | bytes 11534336 | tf_op jit(solution)/shard_map/all_to_all | solution.py:33
  260.0 0.9 broadcast_in_dim.63
  260.9 3.5 %all-to-all-start.1 = ((bf16[4,32,2048]{2,1,0:T(8,128)(2,1)}), bf16[4,32,2048]{2,1,0:T(8,128)(2,1)S(1)}, u32[]{:S(2)}, u32[]{:S(2)}) async-start(bf16[4,32,2048]{2,1,0:T(8,128)(2,1)} %broadcast_in_dim.63), calls=%async_computation.1 | async-start | bytes 1048576 | tf_op jit(solution)/shard_map/all_to_all | solution.py:86
  264.4 6.0 %copy.67 = bf16[2,32,1408,32]{2,3,0,1:T(8,128)(2,1)} copy(bf16[2,32,1408,32]{2,3,1,0:T(8,128)(2,1)} %all_to_all.31) | data formatting | bytes 11534336 | tf_op jit(solution)/shard_map/all_to_all | solution.py:33
  270.3 3.2 %all-to-all-done.1 = bf16[4,32,2048]{2,1,0:T(8,128)(2,1)S(1)} async-done(((bf16[4,32,2048]{2,1,0:T(8,128)(2,1)}), bf16[4,32,2048]{2,1,0:T(8,128)(2,1)S(1)}, u32[]{:S(2)}, u32[]{:S(2)}) %all-to-all-start.1) | async-done | bytes 524320 | tf_op jit(solution)/shard_map/all_to_all | solution.py:86
  273.5 4.5 %fusion.2 = f32[128,1408]{1,0:T(8,128)} fusion(bf16[128,2048]{1,0:T(8,128)(2,1)S(1)} %bitcast.512, bf16[2048,2816]{1,0:T(8,128)(2,1)} %all-gather.10.cloned.1.call-done), kind=kOutput, calls=%fused_computation.2 | convolution fusion | flops 738197504 | bytes 7012352 | tf_op jit(solution)/shard_map/dot_general | solution.py:220
  278.1 7.4 %convolution_convert_fusion.1 = bf16[128,2048]{1,0:T(8,128)(2,1)S(1)} fusion(bf16[1408,2048]{0,1:T(8,128)(2,1)} %bitcast.510, bf16[128,2048]{1,0:T(8,128)(2,1)S(1)} %bitcast.513, bf16[2048,2816]{1,0:T(8,128)(2,1)} %all-gather.10.cloned.1.call-done, f32[128,1408]{1,0:T(8,128)} %fusion.2), kind=kOutput, calls=%fused_computation.8 | convolution fusion | flops 1477738496 | bytes 13303808 | tf_op jit(solution)/shard_map/dot_general | solution.py:223
  285.5 10.8 %all_to_all.32 = bf16[4,32,2048]{2,1,0:T(8,128)(2,1)S(1)} all-to-all(bf16[4,32,2048]{2,1,0:T(8,128)(2,1)S(1)} %bitcast.515), channel_id=1, replica_groups=mesh['sp_0'=8,'sp_1'=4,'sp_2'=2,'tp'=4] {'tp'}, dimensions={0} | all-to-all | bytes 1048576 | tf_op jit(solution)/shard_map/all_to_all | solution.py:80
  296.3 0.7 fusion.92
  (85 shorter events, 1.4 us)
Async XLA Ops:
  6.5 125.9 %copy-start = (bf16[512,2048]{1,0:T(8,128)(2,1)S(1)}, bf16[512,2048]{1,0:T(8,128)(2,1)}, u32[]{:S(2)}) copy-start(bf16[512,2048]{1,0:T(8,128)(2,1)} %param.20) | copy-start | bytes 6291460
  6.5 17.3 %copy-start.2 = (bf16[128,512]{1,0:T(8,128)(2,1)S(1)}, bf16[128,512]{1,0:T(8,128)(2,1)}, u32[]{:S(2)}) copy-start(bf16[128,512]{1,0:T(8,128)(2,1)} %param.15) | copy-start | bytes 393220
  6.5 115.7 %all-gather.8.cloned.1.call-start = ((), (), s32[]{:S(2)}) async-start(), calls=%async_computation.7 | async-start | bytes 1179648 | tf_op jit(solution)/shard_map/all_gather | solution.py:57
  11.1 27.1 %copy-start.3 = (f32[128,4,128]{2,1,0:T(4,128)}, f32[128,4,128]{2,1,0:T(4,128)S(1)}, u32[]{:S(2)}) copy-start(f32[128,4,128]{2,1,0:T(4,128)S(1)} %fusion.93) | copy-start | bytes 786436
  18.8 47.1 %copy-start.7 = (f32[4,128]{1,0:T(4,128)}, f32[4,128]{1,0:T(4,128)S(1)}, u32[]{:S(2)}) copy-start(f32[4,128]{1,0:T(4,128)S(1)} %convert_bitcast_fusion.20) | copy-start | bytes 6148
  30.5 17.8 %copy-start.11 = (f32[4,128]{1,0:T(4,128)}, f32[4,128]{1,0:T(4,128)S(1)}, u32[]{:S(2)}) copy-start(f32[4,128]{1,0:T(4,128)S(1)} %get-tuple-element.106) | copy-start | bytes 6148
  30.5 17.8 %copy-start.12 = (f32[4,128]{1,0:T(4,128)}, f32[4,128]{1,0:T(4,128)S(1)}, u32[]{:S(2)}) copy-start(f32[4,128]{1,0:T(4,128)S(1)} %get-tuple-element.107) | copy-start | bytes 6148
  30.5 17.8 %copy-start.13 = (f32[4,128]{1,0:T(4,128)}, f32[4,128]{1,0:T(4,128)S(1)}, u32[]{:S(2)}) copy-start(f32[4,128]{1,0:T(4,128)S(1)} %get-tuple-element.108) | copy-start | bytes 6148
  37.5 0.7 copy-start.4
  38.1 10.2 %copy-start.9 = (f32[4,128]{1,0:T(4,128)}, f32[4,128]{1,0:T(4,128)S(1)}, u32[]{:S(2)}) copy-start(f32[4,128]{1,0:T(4,128)S(1)} %get-tuple-element.105) | copy-start | bytes 6148
  49.4 79.1 %all-gather.6.cloned.1.call-start = ((), (), s32[]{:S(2)}) async-start(), calls=%async_computation.6 | async-start | bytes 1179648 | tf_op jit(solution)/shard_map/all_gather | solution.py:57
  65.9 0.7 copy-start.5
  65.9 11.6 %copy-start.8 = (f32[4,128]{1,0:T(4,128)}, f32[4,128]{1,0:T(4,128)S(1)}, u32[]{:S(2)}) copy-start(f32[4,128]{1,0:T(4,128)S(1)} %convert_bitcast_fusion.22) | copy-start | bytes 6148
  66.6 11.0 %copy-start.10 = (f32[4,128]{1,0:T(4,128)}, f32[4,128]{1,0:T(4,128)S(1)}, u32[]{:S(2)}) copy-start(f32[4,128]{1,0:T(4,128)S(1)} %get-tuple-element.101) | copy-start | bytes 6148
  77.5 0.8 copy-start.1
  77.5 0.8 copy-start.14
  77.5 0.8 copy-start.15
  77.6 0.8 copy-start.16
  79.3 194.2 %all-gather.10.cloned.1.call-start = ((), (), s32[]{:S(2)}) async-start(), calls=%async_computation.8 | async-start | bytes 11714560 | tf_op jit(solution)/shard_map/all_gather | solution.py:16
  82.7 51.2 %all-to-all-start.2 = ((bf16[4,1,1408,32]{2,3,1,0:T(8,128)(2,1)}), bf16[4,1,1408,32]{2,3,1,0:T(8,128)(2,1)}, u32[]{:S(2)}, u32[]{:S(2)}) async-start(bf16[4,1,1408,32]{2,3,1,0:T(8,128)(2,1)} %stack.9), calls=%async_computation.2 | async-start | bytes 720896 | tf_op jit(solution)/shard_map/all_to_all | solution.py:33
  117.3 11.2 %copy-start.18 = (f32[4,128]{1,0:T(4,128)S(1)}, f32[4,128]{1,0:T(4,128)}, u32[]{:S(2)}) copy-start(f32[4,128]{1,0:T(4,128)} %get-tuple-element.87) | copy-start | bytes 6148
  117.3 11.2 %copy-start.19 = (f32[4,128]{1,0:T(4,128)S(1)}, f32[4,128]{1,0:T(4,128)}, u32[]{:S(2)}) copy-start(f32[4,128]{1,0:T(4,128)} %get-tuple-element.88) | copy-start | bytes 6148
  117.3 11.2 %copy-start.20 = (f32[4,128]{1,0:T(4,128)S(1)}, f32[4,128]{1,0:T(4,128)}, u32[]{:S(2)}) copy-start(f32[4,128]{1,0:T(4,128)} %get-tuple-element.89) | copy-start | bytes 6148
  117.3 11.2 %copy-start.21 = (f32[4,128]{1,0:T(4,128)S(1)}, f32[4,128]{1,0:T(4,128)}, u32[]{:S(2)}) copy-start(f32[4,128]{1,0:T(4,128)} %get-tuple-element.90) | copy-start | bytes 6148
  117.3 11.2 %copy-start.22 = (f32[4,128]{1,0:T(4,128)S(1)}, f32[4,128]{1,0:T(4,128)}, u32[]{:S(2)}) copy-start(f32[4,128]{1,0:T(4,128)} %get-tuple-element.91) | copy-start | bytes 6148
  117.3 11.2 %copy-start.23 = (f32[4,128]{1,0:T(4,128)S(1)}, f32[4,128]{1,0:T(4,128)}, u32[]{:S(2)}) copy-start(f32[4,128]{1,0:T(4,128)} %get-tuple-element.92) | copy-start | bytes 6148
  117.3 11.2 %copy-start.24 = (f32[4,128]{1,0:T(4,128)S(1)}, f32[4,128]{1,0:T(4,128)}, u32[]{:S(2)}) copy-start(f32[4,128]{1,0:T(4,128)} %get-tuple-element.93) | copy-start | bytes 6148
  119.5 9.0 %copy-start.6 = (bf16[8,128,128]{2,1,0:T(8,128)(2,1)S(1)}, bf16[8,128,128]{2,1,0:T(8,128)(2,1)}, u32[]{:S(2)}) copy-start(bf16[8,128,128]{2,1,0:T(8,128)(2,1)} %copy-done.5) | copy-start | bytes 786436
  120.9 11.3 %copy-start.25 = (f32[128]{0:T(128)S(1)}, f32[128]{0:T(128)}, u32[]{:S(2)}) copy-start(f32[128]{0:T(128)} %convert_element_type.813) | copy-start | bytes 1540
  133.8 18.2 %copy-start.17 = (bf16[2048]{0:T(1024)(128)(2,1)S(1)}, bf16[2048]{0:T(1024)(128)(2,1)}, u32[]{:S(2)}) copy-start(bf16[2048]{0:T(1024)(128)(2,1)} %param.22) | copy-start | bytes 12292
  147.5 84.5 %all-to-all-start.3 = ((bf16[8,4,1408,32]{2,3,1,0:T(8,128)(2,1)}), bf16[8,4,1408,32]{2,3,1,0:T(8,128)(2,1)}, u32[]{:S(2)}, u32[]{:S(2)}) async-start(bf16[8,4,1408,32]{2,3,1,0:T(8,128)(2,1)} %stack.10), calls=%async_computation.3 | async-start | bytes 5767168 | tf_op jit(solution)/shard_map/all_to_all | solution.py:33
  260.9 12.6 %all-to-all-start.1 = ((bf16[4,32,2048]{2,1,0:T(8,128)(2,1)}), bf16[4,32,2048]{2,1,0:T(8,128)(2,1)S(1)}, u32[]{:S(2)}, u32[]{:S(2)}) async-start(bf16[4,32,2048]{2,1,0:T(8,128)(2,1)} %broadcast_in_dim.63), calls=%async_computation.1 | async-start | bytes 1048576 | tf_op jit(solution)/shard_map/all_to_all | solution.py:86
Sparse Core Ops, SparseCore 0:
  49.5 37.8 all-gather.7
  89.1 36.8 all-gather.5
  128.7 122.8 all-gather.9
